TPU v7x, 256 devices: a whole 4x4x8 slice. The times are simulated.
256 devices in a mesh: sp: 64 (over z, y, core), tp: 4 (over x).
Axes of the slice: x: 4, y: 4, z: 8, core: 2. Of those that a mesh axis runs over, the one named last changes fastest.
Arguments:
- tokens: bfloat16 [49152, 2048], P('sp'), may hold values from -6 to 6
- input_gain: bfloat16 [2048], replicated, may hold values from 0.099609375 to 1.8984375
- gate_weight: bfloat16 [2048, 2048], P('sp', 'tp'), may hold values from -0.125 to 0.125
- value_weight: bfloat16 [2048, 2048], P('sp', 'tp'), may hold values from -0.125 to 0.125
- inflow_weight: bfloat16 [2048, 4, 128], P('sp', 'tp'), may hold values from -0.125 to 0.125
- readout_weight: bfloat16 [2048, 4, 128], P('sp', 'tp'), may hold values from -0.125 to 0.125
- step_weight: bfloat16 [2048, 2, 32], P('sp', None, 'tp'), may hold values from -0.125 to 0.125
- conv_values: bfloat16 [5, 2048], P(None, 'tp'), may hold values from -2.5 to 2.5
- conv_inflow: bfloat16 [5, 4, 128], P(None, 'tp'), may hold values from -2.5 to 2.5
- conv_readout: bfloat16 [5, 4, 128], P(None, 'tp'), may hold values from -2.5 to 2.5
- log_rate: float32 [2, 49152, 32], P(None, 'sp', 'tp'), may hold values from -20 to 0
- group_gain: bfloat16 [2048], P('tp'), may hold values from 0.099609375 to 1.8984375
- query_weight: bfloat16 [2048, 2048], P('sp', 'tp'), may hold values from -8 to 8
- key_weight: bfloat16 [2048, 512], P('sp', 'tp'), may hold values from -8 to 8
- vector_weight: bfloat16 [2048, 512], P('sp', 'tp'), may hold values from -0.125 to 0.125
- sink_logit: float32 [32], P('tp'), may hold values from 3 to 7
- state_out: bfloat16 [2048, 2048], P('tp', 'sp'), may hold values from -0.125 to 0.125
- window_out: bfloat16 [2048, 2048], P('tp', 'sp'), may hold values from -1 to 1
Outputs:
- mixed: bfloat16 [49152, 2048], P('sp', 'tp')
- log_total: float32 [49152, 32], P('sp', 'tp')
All inputs are finite; a program needn't handle non-finite values.
Results may differ from a plain program's by a relative error of at most 0.015.
The roundings to bfloat16 on the way count: a program that leaves them out, or rounds other values in their place, can miss the bound.
Values may be sent and summed in bfloat16 or wider, within the bound.
No kernel may reach another device: no remote copies, remote signals or barrier semaphores. Data moves between devices by JAX's collectives and lax.ppermute only.
A program may use at most 128 MiB of HBM per device.

v0:
```python
import jax
import jax.numpy as jnp
from jax import lax
from jax.sharding import Mesh
from jax.sharding import PartitionSpec as P

HEAD_DIM = 64
CONV = 5
SSD_BLOCK = 128
WINDOW = 128
QBLOCK = 256
GRID_W = 64
SP = ("sp_0", "sp_1", "sp_2")
EPS = 1e-06
ROPE_BASE = 10000.0
HIGH = lax.Precision.HIGH


def turned_gather(arrays, axis, dims):
    turned = [jnp.moveaxis(a, dim, 0) for a, dim in zip(arrays, dims)]
    widths = [t[0].size for t in turned]
    both = jnp.concatenate([t.reshape(-1, w) for t, w in zip(turned, widths)], axis=1)
    out = lax.all_gather(both, axis, axis=0, tiled=True)
    parts = jnp.split(out, [sum(widths[:k]) for k in range(1, len(widths))], axis=1)
    return tuple(
        (
            jnp.moveaxis(b.reshape(-1, *t.shape[1:]), 0, dim)
            for b, t, dim in zip(parts, turned, dims)
        )
    )


def nothing_yet(value, identity):
    return jax.tree.map(
        lambda part, zero: jnp.zeros_like(part) + jnp.asarray(zero, part.dtype), value, identity
    )


def carried_in(value, axes, combine, identity, reverse):
    before = start = nothing_yet(value, identity)
    running = value
    for axis in reversed(axes):
        length, position = (lax.axis_size(axis), lax.axis_index(axis))
        pieces = jax.tree.map(
            lambda part, kind: lax.all_gather(part.astype(kind), axis),
            running,
            jax.tree.map(lambda a: jnp.bfloat16 if a.dtype == jnp.float32 else a.dtype, value),
        )
        inside, running = (start, start)
        for k in reversed(range(length)) if reverse else range(length):
            passed = k > position if reverse else k < position
            running = combine(
                running, jax.tree.map(lambda part, own: part[k].astype(own.dtype), pieces, value)
            )
            inside = jax.tree.map(lambda new, old: jnp.where(passed, new, old), running, inside)
        before = combine(inside, before)
    return before


def with_halo(cells, sides, width):
    for axis, dim in sides:
        count = lax.axis_size(axis)
        ends = count - 1
        head = lax.slice_in_dim(cells, 0, width, axis=dim)
        tail = lax.slice_in_dim(cells, cells.shape[dim] - width, cells.shape[dim], axis=dim)
        cells = jnp.concatenate(
            [
                lax.ppermute(tail, axis, [(i, (i + 1) % count) for i in range(ends)]),
                cells,
                lax.ppermute(head, axis, [((i + 1) % count, i) for i in range(ends)]),
            ],
            axis=dim,
        )
    return cells


def cut_along(value, dim, length):
    shape = value.shape
    parts = value.reshape(*shape[:dim], length, shape[dim] // length, *shape[dim + 1 :])
    return jnp.moveaxis(parts, dim, 0)


def sent_and_summed(value, axis, dim):
    parts = cut_along(value, dim, lax.axis_size(axis))
    arrived = lax.all_to_all(parts, axis, split_axis=0, concat_axis=0, tiled=True)
    return arrived.astype(jnp.float32).sum(axis=0)


def rope_pairs(part, angle):
    half = part.shape[-1] // 2
    cosine = jnp.cos(angle)[:, None, :]
    sine = jnp.sin(angle)[:, None, :]
    first = part[..., :half]
    second = part[..., half:]
    return jnp.concatenate(
        [first * cosine - second * sine, second * cosine + first * sine], axis=-1
    )


def axial_rope(heads, positions):
    width = heads.shape[-1]
    quarter = width // 4
    freqs = ROPE_BASE ** (-jnp.arange(quarter).astype(jnp.float32) / quarter)
    row_angle = (positions // GRID_W).astype(jnp.float32)[:, None] * freqs
    col_angle = (positions % GRID_W).astype(jnp.float32)[:, None] * freqs
    half = width // 2
    wide = heads.astype(jnp.float32)
    turned = jnp.concatenate(
        [rope_pairs(wide[..., :half], row_angle), rope_pairs(wide[..., half:], col_angle)], axis=-1
    )
    return turned.astype(jnp.bfloat16)


def block_ssd(state, inputs):
    xdt, decay, inflow, readout = inputs
    length = decay.shape[0]
    heads = xdt.shape[1]
    groups = inflow.shape[1]
    repeat = heads // groups
    cum = jnp.cumsum(decay, axis=0)
    seg = cum[:, None, :] - cum[None, :, :]
    lower = jnp.arange(length)[:, None] >= jnp.arange(length)[None, :]
    weight = jnp.exp(jnp.where(lower[:, :, None], seg, -jnp.inf))
    intersection = jnp.einsum("lgn,sgn->lsg", readout, inflow, preferred_element_type=jnp.float32)
    intersection = jnp.repeat(intersection, repeat, axis=2)
    final_result = jnp.einsum("lsh,shp->lhp", intersection * weight, xdt, precision=HIGH)
    read_heads = jnp.repeat(readout, repeat, axis=1).astype(jnp.float32)
    final_result = final_result + jnp.exp(cum)[:, :, None] * jnp.einsum(
        "lhn,hpn->lhp", read_heads, state, precision=HIGH
    )
    write_heads = jnp.repeat(inflow, repeat, axis=1).astype(jnp.float32)
    to_end = jnp.exp(cum[-1][None, :] - cum)
    fresh = jnp.einsum("shp,shn->hpn", xdt * to_end[:, :, None], write_heads, precision=HIGH)
    return (jnp.exp(cum[-1])[:, None, None] * state + fresh, final_result)


def chain(earlier, later):
    return (earlier[0] + later[0], jnp.exp(later[0])[:, None, None] * earlier[1] + later[1])


def flatten_rows(weight):
    return weight.reshape(weight.shape[0], -1)


def shards(
    tokens,
    input_gain,
    gate_weight,
    value_weight,
    inflow_weight,
    readout_weight,
    step_weight,
    conv_values,
    conv_inflow,
    conv_readout,
    log_rate,
    group_gain,
    query_weight,
    key_weight,
    vector_weight,
    sink_logit,
    state_out,
    window_out,
):
    count = tokens.shape[0]
    offset = lax.axis_index(SP) * count
    seq_total = count * lax.axis_size(SP)
    positions = offset + jnp.arange(count, dtype=jnp.int32)
    heads = step_weight.shape[2]
    groups = inflow_weight.shape[1]
    state_len = inflow_weight.shape[2]
    inner_local = value_weight.shape[1]
    q_count = query_weight.shape[1] // HEAD_DIM
    kv_count = key_weight.shape[1] // HEAD_DIM
    kv_width = key_weight.shape[1]
    wide = tokens.astype(jnp.float32)
    normed = (
        wide
        * lax.rsqrt(jnp.mean(wide * wide, axis=1, keepdims=True) + EPS)
        * input_gain.astype(jnp.float32)
    ).astype(jnp.bfloat16)
    out_stack = jnp.concatenate([state_out, window_out], axis=0)
    gathered = turned_gather(
        (
            gate_weight,
            value_weight,
            inflow_weight,
            readout_weight,
            step_weight,
            query_weight,
            key_weight,
            vector_weight,
            out_stack,
        ),
        SP,
        (0, 0, 0, 0, 0, 0, 0, 0, 1),
    )
    pieces = gathered[:8]
    matrices = (
        pieces[0],
        jnp.concatenate([pieces[1], flatten_rows(pieces[2]), flatten_rows(pieces[3])], axis=1),
        flatten_rows(pieces[4]),
        pieces[5],
        jnp.concatenate([pieces[6], pieces[7]], axis=1),
    )
    sums = tuple(
        (jnp.dot(normed, matrix, preferred_element_type=jnp.float32) for matrix in matrices)
    )
    out_whole = gathered[8]
    gate = sums[0].astype(jnp.bfloat16)
    conv_input = sums[1].astype(jnp.bfloat16)
    step = jax.nn.softplus(sums[2]).reshape(count, 2, heads)
    queries = sums[3].astype(jnp.bfloat16)
    keyvals = sums[4].astype(jnp.bfloat16)

    def direction(xdt, decay, inflow, readout, backward):
        if backward:
            xdt = jnp.flip(xdt, 0)
            decay = jnp.flip(decay, 0)
            inflow = jnp.flip(inflow, 0)
            readout = jnp.flip(readout, 0)
        blocks = count // SSD_BLOCK
        start_state = jnp.zeros((heads, HEAD_DIM, state_len), jnp.float32)
        shaped = (
            xdt.reshape(blocks, SSD_BLOCK, heads, HEAD_DIM),
            decay.reshape(blocks, SSD_BLOCK, heads),
            inflow.reshape(blocks, SSD_BLOCK, groups, state_len),
            readout.reshape(blocks, SSD_BLOCK, groups, state_len),
        )
        end_state, local = lax.scan(block_ssd, start_state, shaped)
        local = local.reshape(count, heads, HEAD_DIM)
        summary = (jnp.sum(decay, axis=0), end_state)
        identity = (jnp.zeros((heads,), jnp.float32), jnp.zeros_like(end_state))
        if backward:
            incoming = carried_in(summary, SP, chain, identity, True)
        else:
            incoming = carried_in(summary, SP, chain, identity, False)
        reach = jnp.exp(jnp.cumsum(decay, axis=0))
        per_head = jnp.repeat(readout, heads // groups, axis=1).astype(jnp.float32)
        local = local + reach[:, :, None] * jnp.einsum(
            "lhn,hpn->lhp", per_head, incoming[1], precision=HIGH
        )
        if backward:
            local = jnp.flip(local, 0)
        return local

    reach_rows = CONV // 2
    padded = with_halo(conv_input, ((SP, 0),), CONV // 2).astype(jnp.float32)
    taps = jnp.concatenate(
        [conv_values, flatten_rows(conv_inflow), flatten_rows(conv_readout)], axis=1
    ).astype(jnp.float32)
    conv_sum = padded[0:count] * taps[0]
    for tap in range(1, 2 * reach_rows + 1):
        conv_sum = conv_sum + padded[tap : tap + count] * taps[tap]
    conv_short = jax.nn.silu(conv_sum).astype(jnp.bfloat16)
    conv_out = conv_short.astype(jnp.float32)
    split_mid = inner_local + groups * state_len
    xs = conv_out[:, :inner_local].reshape(count, heads, HEAD_DIM)
    inflow = conv_short[:, inner_local:split_mid].reshape(count, groups, state_len)
    readout = conv_short[:, split_mid:].reshape(count, groups, state_len)
    decay = -jnp.exp(log_rate) * jnp.transpose(step, (1, 0, 2))
    forward = direction(xs * step[:, 0, :, None], decay[0], inflow, readout, False)
    backward = direction(xs * step[:, 1, :, None], decay[1], inflow, readout, True)
    combined = (forward + backward).reshape(count, -1) * jax.nn.silu(gate.astype(jnp.float32))
    grouped = combined.reshape(count, groups, -1)
    grouped = grouped * lax.rsqrt(jnp.mean(grouped * grouped, axis=2, keepdims=True) + EPS)
    state_features = (grouped.reshape(count, -1) * group_gain.astype(jnp.float32)).astype(
        jnp.bfloat16
    )
    q_heads = axial_rope(queries.reshape(count, q_count, HEAD_DIM), positions)
    k_heads = axial_rope(keyvals[:, :kv_width].reshape(count, kv_count, HEAD_DIM), positions)
    both = jnp.concatenate([k_heads.reshape(count, -1), keyvals[:, kv_width:]], axis=1)
    beside_all = with_halo(both, ((SP, 0),), WINDOW)
    repeat = q_count // kv_count
    band = QBLOCK + 2 * WINDOW
    sinks = sink_logit.reshape(kv_count, repeat, 1, 1)
    grouped_q = q_heads.reshape(count, kv_count, repeat, HEAD_DIM)

    def attend(index):
        start = index * QBLOCK
        block_q = lax.dynamic_slice_in_dim(grouped_q, start, QBLOCK, 0)
        block_kv = lax.dynamic_slice_in_dim(beside_all, start, band, 0)
        block_k = block_kv[:, :kv_width].reshape(band, kv_count, HEAD_DIM)
        block_v = block_kv[:, kv_width:].reshape(band, kv_count, HEAD_DIM)
        scores = jnp.einsum(
            "qkrd,skd->krqs", block_q, block_k, preferred_element_type=jnp.float32
        ) * HEAD_DIM ** (-0.5)
        query_pos = offset + start + jnp.arange(QBLOCK, dtype=jnp.int32)
        key_pos = offset + start - WINDOW + jnp.arange(band, dtype=jnp.int32)
        valid = (
            (jnp.abs(query_pos[:, None] - key_pos[None, :]) <= WINDOW)
            & (key_pos >= 0)[None, :]
            & (key_pos < seq_total)[None, :]
        )
        scores = jnp.where(valid, scores, -jnp.inf)
        top = jnp.maximum(jnp.max(scores, axis=-1, keepdims=True), sinks)
        expo = jnp.exp(scores - top)
        total = jnp.sum(expo, axis=-1, keepdims=True) + jnp.exp(sinks - top)
        probs = expo.astype(jnp.bfloat16)
        values = jnp.einsum("krqs,skd->qkrd", probs, block_v, preferred_element_type=jnp.float32)
        values = values / jnp.transpose(total, (2, 0, 1, 3))
        logs = jnp.transpose((top + jnp.log(total))[..., 0], (2, 0, 1)).reshape(QBLOCK, -1)
        return (values.astype(jnp.bfloat16).reshape(QBLOCK, -1), logs)

    feats, logs = lax.map(attend, jnp.arange(count // QBLOCK, dtype=jnp.int32))
    window_features = feats.reshape(count, -1)
    log_total = logs.reshape(count, -1)
    features = jnp.concatenate([state_features, window_features], axis=1)
    terms = jnp.dot(features, out_whole, preferred_element_type=jnp.float32)
    mixed = sent_and_summed(terms.astype(jnp.bfloat16), "tp", 1).astype(jnp.bfloat16)
    return (mixed, log_total)


def solution(mesh):
    torus = Mesh(mesh.devices.reshape(8, 4, 2, mesh.shape["tp"]), ("sp_0", "sp_1", "sp_2", "tp"))
    return jax.shard_map(
        shards,
        mesh=torus,
        in_specs=(
            P(SP, None),
            P(),
            P(SP, "tp"),
            P(SP, "tp"),
            P(SP, "tp", None),
            P(SP, "tp", None),
            P(SP, None, "tp"),
            P(None, "tp"),
            P(None, "tp", None),
            P(None, "tp", None),
            P(None, SP, "tp"),
            P("tp"),
            P(SP, "tp"),
            P(SP, "tp"),
            P(SP, "tp"),
            P("tp"),
            P("tp", SP),
            P("tp", SP),
        ),
        out_specs=(P(SP, "tp"), P(SP, "tp")),
        check_vma=False,
    )
```

profile of v0, /device:TPU:8, one launch (start us, length us, event | category | flops | bytes accessed | tf_op | source)
XLA Modules:
  0.0 523.0 jit_solution(13843516485455394829)
XLA Ops:
  19.3 83.6 %all-gather.12.cloned.1.call-done = bf16[2048,3088]{1,0:T(8,128)(2,1)} async-done(((bf16[32,3088]{1,0:T(8,128)(2,1)}), bf16[2048,3088]{1,0:T(8,128)(2,1)}) %all-gather.12.cloned.1.call-update) | async-done | bytes 12648464 | tf_op jit(solution)/shard_map/all_gather | solution.py:23
  121.5 5.5 %fusion.101 = bf16[768,768]{1,0:T(8,128)(2,1)S(1)} fusion(bf16[2048,3088]{1,0:T(8,128)(2,1)} %all-gather.12.cloned.1.call-done, bf16[768,2048]{1,0:T(8,128)(2,1)} %param.24, f32[2048]{0:T(1024)S(1)} %convert_element_type.661, f32[768]{0:T(1024)S(1)} %add_rsqrt_fusion.1), kind=kOutput, calls=%fused_computation.141 | convolution fusion | flops 2422800384 | bytes 7482368 | tf_op jit(solution)/shard_map/dot_general | solution.py:207
  139.2 10.6 %all-gather.6 = bf16[4,1,8]{2,1,0:T(2,128)(2,1)S(1)} all-gather(bf16[1,1,8]{2,1,0:T(2,128)(2,1)S(1)} %get-tuple-element.405), channel_id=1, replica_groups=mesh['sp_0'=8,'sp_1'=4,'sp_2'=2,'tp'=4] {'sp_1'}, dimensions={0}, use_global_device_ids=true | all-gather | bytes 80 | tf_op jit(solution)/shard_map/all_gather | solution.py:45
  151.5 16.1 %all-gather.7 = bf16[8,1,8]{2,1,0:T(2,128)(2,1)S(1)} all-gather(bf16[1,1,8]{2,1,0:T(2,128)(2,1)S(1)} %get-tuple-element.396), channel_id=1, replica_groups=mesh['sp_0'=8,'sp_1'=4,'sp_2'=2,'tp'=4] {'sp_0'}, dimensions={0}, use_global_device_ids=true | all-gather | bytes 144 | tf_op jit(solution)/shard_map/all_gather | solution.py:45
  171.6 10.2 %all-gather.4 = bf16[4,1,8]{2,1,0:T(2,128)(2,1)S(1)} all-gather(bf16[1,1,8]{2,1,0:T(2,128)(2,1)S(1)} %get-tuple-element.402), channel_id=1, replica_groups=mesh['sp_0'=8,'sp_1'=4,'sp_2'=2,'tp'=4] {'sp_1'}, dimensions={0}, use_global_device_ids=true | all-gather | bytes 80 | tf_op jit(solution)/shard_map/all_gather | solution.py:45
  183.6 13.5 %all-gather.5 = bf16[8,1,8]{2,1,0:T(2,128)(2,1)S(1)} all-gather(bf16[1,1,8]{2,1,0:T(2,128)(2,1)S(1)} %get-tuple-element.391), channel_id=1, replica_groups=mesh['sp_0'=8,'sp_1'=4,'sp_2'=2,'tp'=4] {'sp_0'}, dimensions={0}, use_global_device_ids=true | all-gather | bytes 144 | tf_op jit(solution)/shard_map/all_gather | solution.py:45
  222.3 74.4 %while.42 = (s32[]{:T(128)}, f32[8,64,128]{2,1,0:T(8,128)S(1)}, f32[6,128,8,64]{1,0,3,2:T(8,128)S(1)}, f32[6,128,8]{2,1,0:T(8,128)}, f32[6,128,8,64]{1,0,3,2:T(8...) while((s32[]{:T(128)}, f32[8,64,128]{2,1,0:T(8,128)S(1)}, ...), condition=%wide.region_9.10_spmd.clone, body=%wide.region_7.9_spmd.clone.sunk | while | flops 156188672 | bytes 3768652 | solution.py:230
  229.6 5.1 dynamic_update_slice.32
  242.0 5.1 dynamic_update_slice.32
  254.4 5.1 dynamic_update_slice.32
  266.8 5.1 dynamic_update_slice.32
  299.6 11.9 %all_gather.68 = bf16[4,8,64,128]{3,2,1,0:T(8,128)(2,1)S(1)} all-gather(bf16[1,8,64,128]{3,2,1,0:T(8,128)(2,1)S(1)} %fusion.172), channel_id=1, replica_groups=mesh['sp_0'=8,'sp_1'=4,'sp_2'=2,'tp'=4] {'sp_1'}, dimensions={0}, use_global_device_ids=true | all-gather | bytes 655360 | tf_op jit(solution)/shard_map/all_gather | solution.py:45
  318.4 80.1 %while.41 = (s32[]{:T(128)}, f32[8,64,128]{2,1,0:T(8,128)S(1)}, f32[6,128,8,64]{1,0,3,2:T(8,128)}, f32[6,128,8]{2,1,0:T(8,128)}, f32[6,128,8,64]{1,0,3,2:T(8,128...) while((s32[]{:T(128)}, f32[8,64,128]{2,1,0:T(8,128)S(1)}, ...), condition=%wide.region_3.4_spmd.clone, body=%wide.region_1.3_spmd.clone.sunk | while | flops 156188672 | bytes 3768652 | solution.py:230
  324.1 7.7 %dynamic_update_slice.31 = f32[6,128,8,64]{1,0,3,2:T(8,128)} dynamic-update-slice(f32[6,128,8,64]{1,0,3,2:T(8,128)} %get-tuple-element.665, f32[1,128,8,64]{1,0,3,2:T(1,128)S(1)} %bitcast.674, s32[]{:T(128)S(6)} %copy.178, s32[]{:T(128)} %constant.172.clone.1..sunk.1, s32[]{:T(128)} %constant.172.clone.1..sunk.1, s32[]{:T(128)} %constant.172.clone.1..sunk.1) | dynamic-update-slice | bytes 524292 | tf_op jit(solution)/shard_map/while/body/jit(dynamic_update_index_in_dim)/dynamic_update_slice | solution.py:230
  337.4 7.7 %dynamic_update_slice.31 = f32[6,128,8,64]{1,0,3,2:T(8,128)} dynamic-update-slice(f32[6,128,8,64]{1,0,3,2:T(8,128)} %get-tuple-element.665, f32[1,128,8,64]{1,0,3,2:T(1,128)S(1)} %bitcast.674, s32[]{:T(128)S(6)} %copy.178, s32[]{:T(128)} %constant.172.clone.1..sunk.1, s32[]{:T(128)} %constant.172.clone.1..sunk.1, s32[]{:T(128)} %constant.172.clone.1..sunk.1) | dynamic-update-slice | bytes 524292 | tf_op jit(solution)/shard_map/while/body/jit(dynamic_update_index_in_dim)/dynamic_update_slice | solution.py:230
  350.8 7.7 %dynamic_update_slice.31 = f32[6,128,8,64]{1,0,3,2:T(8,128)} dynamic-update-slice(f32[6,128,8,64]{1,0,3,2:T(8,128)} %get-tuple-element.665, f32[1,128,8,64]{1,0,3,2:T(1,128)S(1)} %bitcast.674, s32[]{:T(128)S(6)} %copy.178, s32[]{:T(128)} %constant.172.clone.1..sunk.1, s32[]{:T(128)} %constant.172.clone.1..sunk.1, s32[]{:T(128)} %constant.172.clone.1..sunk.1) | dynamic-update-slice | bytes 524292 | tf_op jit(solution)/shard_map/while/body/jit(dynamic_update_index_in_dim)/dynamic_update_slice | solution.py:230
  364.1 7.7 %dynamic_update_slice.31 = f32[6,128,8,64]{1,0,3,2:T(8,128)} dynamic-update-slice(f32[6,128,8,64]{1,0,3,2:T(8,128)} %get-tuple-element.665, f32[1,128,8,64]{1,0,3,2:T(1,128)S(1)} %bitcast.674, s32[]{:T(128)S(6)} %copy.178, s32[]{:T(128)} %constant.172.clone.1..sunk.1, s32[]{:T(128)} %constant.172.clone.1..sunk.1, s32[]{:T(128)} %constant.172.clone.1..sunk.1) | dynamic-update-slice | bytes 524292 | tf_op jit(solution)/shard_map/while/body/jit(dynamic_update_index_in_dim)/dynamic_update_slice | solution.py:230
  377.5 7.7 %dynamic_update_slice.31 = f32[6,128,8,64]{1,0,3,2:T(8,128)} dynamic-update-slice(f32[6,128,8,64]{1,0,3,2:T(8,128)} %get-tuple-element.665, f32[1,128,8,64]{1,0,3,2:T(1,128)S(1)} %bitcast.674, s32[]{:T(128)S(6)} %copy.178, s32[]{:T(128)} %constant.172.clone.1..sunk.1, s32[]{:T(128)} %constant.172.clone.1..sunk.1, s32[]{:T(128)} %constant.172.clone.1..sunk.1) | dynamic-update-slice | bytes 524292 | tf_op jit(solution)/shard_map/while/body/jit(dynamic_update_index_in_dim)/dynamic_update_slice | solution.py:230
  390.8 7.7 %dynamic_update_slice.31 = f32[6,128,8,64]{1,0,3,2:T(8,128)} dynamic-update-slice(f32[6,128,8,64]{1,0,3,2:T(8,128)} %get-tuple-element.665, f32[1,128,8,64]{1,0,3,2:T(1,128)S(1)} %bitcast.674, s32[]{:T(128)S(6)} %copy.178, s32[]{:T(128)} %constant.172.clone.1..sunk.1, s32[]{:T(128)} %constant.172.clone.1..sunk.1, s32[]{:T(128)} %constant.172.clone.1..sunk.1) | dynamic-update-slice | bytes 524292 | tf_op jit(solution)/shard_map/while/body/jit(dynamic_update_index_in_dim)/dynamic_update_slice | solution.py:230
  402.0 13.7 %all_gather.61 = bf16[4,8,64,128]{3,2,1,0:T(8,128)(2,1)S(1)} all-gather(bf16[1,8,64,128]{3,2,1,0:T(8,128)(2,1)S(1)} %fusion.168), channel_id=1, replica_groups=mesh['sp_0'=8,'sp_1'=4,'sp_2'=2,'tp'=4] {'sp_1'}, dimensions={0}, use_global_device_ids=true | all-gather | bytes 655360 | tf_op jit(solution)/shard_map/all_gather | solution.py:45
  422.7 19.3 %while.40 = (s32[]{:T(128)}, bf16[3,256,512]{2,1,0:T(8,128)(2,1)S(1)}, f32[3,256,8]{1,2,0:T(8,128)}, s32[3]{0:T(128)S(1)}, bf16[1024,256]{0,1:T(8,128)(2,1)S(1)}...) while((s32[]{:T(128)}, ...), condition=%wide.region_17.18_spmd, body=%wide.region_14.17_spmd.sunk | while | flops 280901888 | bytes 15614348 | solution.py:305
  453.0 7.5 %all-gather.14.cloned.1.call-done = bf16[8,8,64,128]{3,2,1,0:T(8,128)(2,1)} async-done(((bf16[1,8,64,128]{3,2,1,0:T(8,128)(2,1)}), bf16[8,8,64,128]{3,2,1,0:T(8,128)(2,1)}) %all-gather.14.cloned.1.call-update) | async-done | bytes 1048592 | tf_op jit(solution)/shard_map/all_gather | solution.py:45
  469.1 8.7 %fusion.78 = bf16[768,2048]{1,0:T(8,128)(2,1)S(1)} fusion(bf16[2048,3088]{1,0:T(8,128)(2,1)} %all-gather.12.cloned.1.call-done, bf16[768,512]{0,1:T(8,128)(2,1)S(1)} %copy-done.11, bf16[768,512]{0,1:T(8,128)(2,1)S(1)} %multiply_convert_fusion.1), kind=kOutput, calls=%fused_computation.107 | convolution fusion | flops 3225944064 | bytes 8912896 | tf_op jit(solution)/shard_map/dot_general | solution.py:309
  478.1 36.8 %all_to_all.5 = bf16[4,768,512]{2,1,0:T(8,128)(2,1)S(1)} all-to-all(bf16[4,768,512]{2,1,0:T(8,128)(2,1)S(1)} %bitcast.677), channel_id=1, replica_groups=mesh['sp_0'=8,'sp_1'=4,'sp_2'=2,'tp'=4] {'tp'}, dimensions={0} | all-to-all | bytes 6291456 | tf_op jit(solution)/shard_map/all_to_all | solution.py:85
  (455 shorter events, 220.0 us)
Async XLA Ops:
  7.2 95.8 %all-gather.12.cloned.1.call-start = ((), (), s32[]{:S(2)}) async-start(), calls=%async_computation.1 | async-start | bytes 13312000 | tf_op jit(solution)/shard_map/all_gather | solution.py:23
  10.4 432.7 %all-gather.16.cloned.1.call-start = ((), (), s32[]{:S(2)}) async-start(), calls=%async_computation.3 | async-start | bytes 1179648 | tf_op jit(solution)/shard_map/all_gather | solution.py:45
  18.9 102.6 %copy-start.16 = (f32[768]{0:T(1024)}, f32[768]{0:T(1024)S(1)}, u32[]{:S(2)}) copy-start(f32[768]{0:T(1024)S(1)} %add_rsqrt_fusion.1) | copy-start | bytes 9220
  107.9 313.6 %collective-permute-start.3 = (bf16[128,256]{0,1:T(8,128)(2,1)}, bf16[128,256]{0,1:T(8,128)(2,1)}, u32[]{:S(2)}, u32[]{:S(2)}) collective-permute-start(bf16[128,256]{0,1:T(8,128)(2,1)} %get-tuple-element.360), channel_id=1, source_target_pairs={{4,0},{8,4},{12,8},{16,12},{20,16},{24,20},{28,24},{32,28},{36,32}... | collective-permute-start | bytes 196616 | tf_op jit(solution)/shard_map/ppermute | solution.py:70
  111.4 310.1 %collective-permute-start.2 = (bf16[128,256]{0,1:T(8,128)(2,1)}, bf16[128,256]{0,1:T(8,128)(2,1)}, u32[]{:S(2)}, u32[]{:S(2)}) collective-permute-start(bf16[128,256]{0,1:T(8,128)(2,1)} %get-tuple-element.359), channel_id=1, source_target_pairs={{0,4},{4,8},{8,12},{12,16},{16,20},{20,24},{24,28},{28,32},{32,36}... | collective-permute-start | bytes 196616 | tf_op jit(solution)/shard_map/ppermute | solution.py:68
  127.0 74.1 %collective-permute-start.1 = (bf16[2,768]{1,0:T(2,128)(2,1)S(1)}, bf16[2,768]{1,0:T(2,128)(2,1)S(1)}, u32[]{:S(2)}, u32[]{:S(2)}) collective-permute-start(bf16[2,768]{1,0:T(2,128)(2,1)S(1)} %get-tuple-element.354), channel_id=1, source_target_pairs={{4,0},{8,4},{12,8},{16,12},{20,16},{24,20},{28,24},{32,28},{36,32}... | collective-permute-start | bytes 9224 | tf_op jit(solution)/shard_map/ppermute | solution.py:70
  130.6 70.5 %collective-permute-start = (bf16[2,768]{1,0:T(2,128)(2,1)S(1)}, bf16[2,768]{1,0:T(2,128)(2,1)S(1)}, u32[]{:S(2)}, u32[]{:S(2)}) collective-permute-start(bf16[2,768]{1,0:T(2,128)(2,1)S(1)} %get-tuple-element.353), channel_id=1, source_target_pairs={{0,4},{4,8},{8,12},{12,16},{16,20},{20,24},{24,28},{28,32},{32,36}... | collective-permute-start | bytes 9224 | tf_op jit(solution)/shard_map/ppermute | solution.py:68
  313.8 146.7 %all-gather.14.cloned.1.call-start = ((), (), s32[]{:S(2)}) async-start(), calls=%async_computation.2 | async-start | bytes 1179648 | tf_op jit(solution)/shard_map/all_gather | solution.py:45
  422.5 20.7 %copy-start.7 = (bf16[16,64,128]{2,1,0:T(8,128)(2,1)S(1)}, bf16[16,64,128]{2,1,0:T(8,128)(2,1)}, u32[]{:S(2)}) copy-start(bf16[16,64,128]{2,1,0:T(8,128)(2,1)} %copy-done.6) | copy-start | bytes 786436
  422.5 20.7 %copy-start.13 = (f32[768,8]{0,1:T(8,128)S(1)}, f32[768,8]{0,1:T(8,128)}, u32[]{:S(2)}) copy-start(f32[768,8]{0,1:T(8,128)} %exponential_bitcast_fusion) | copy-start | bytes 73732
  422.5 20.7 %copy-start.20 = (f32[8]{0:T(128)S(1)}, f32[8]{0:T(128)}, u32[]{:S(2)}) copy-start(f32[8]{0:T(128)} %get-tuple-element.404) | copy-start | bytes 100
  422.5 20.6 %copy-start.21 = (f32[8]{0:T(128)S(1)}, f32[8]{0:T(128)}, u32[]{:S(2)}) copy-start(f32[8]{0:T(128)} %get-tuple-element.406) | copy-start | bytes 100
  422.5 20.6 %copy-start.23 = (f32[8]{0:T(128)S(1)}, f32[8]{0:T(128)}, u32[]{:S(2)}) copy-start(f32[8]{0:T(128)} %get-tuple-element.397) | copy-start | bytes 100
  422.5 20.6 %copy-start.27 = (f32[8]{0:T(128)S(1)}, f32[8]{0:T(128)}, u32[]{:S(2)}) copy-start(f32[8]{0:T(128)} %get-tuple-element.398) | copy-start | bytes 100
  422.6 20.6 %copy-start.28 = (f32[8]{0:T(128)S(1)}, f32[8]{0:T(128)}, u32[]{:S(2)}) copy-start(f32[8]{0:T(128)} %get-tuple-element.399) | copy-start | bytes 100
  422.6 20.6 %copy-start.29 = (f32[8]{0:T(128)S(1)}, f32[8]{0:T(128)}, u32[]{:S(2)}) copy-start(f32[8]{0:T(128)} %get-tuple-element.400) | copy-start | bytes 100
  422.6 20.6 %copy-start.31 = (f32[8]{0:T(128)S(1)}, f32[8]{0:T(128)}, u32[]{:S(2)}) copy-start(f32[8]{0:T(128)} %get-tuple-element.329) | copy-start | bytes 100
  422.6 20.6 %copy-start.40 = (f32[8]{0:T(128)S(1)}, f32[8]{0:T(128)}, u32[]{:S(2)}) copy-start(f32[8]{0:T(128)} %get-tuple-element.383) | copy-start | bytes 100
  422.6 20.6 %copy-start.41 = (f32[8]{0:T(128)S(1)}, f32[8]{0:T(128)}, u32[]{:S(2)}) copy-start(f32[8]{0:T(128)} %get-tuple-element.384) | copy-start | bytes 100
  422.6 20.6 %copy-start.42 = (f32[8]{0:T(128)S(1)}, f32[8]{0:T(128)}, u32[]{:S(2)}) copy-start(f32[8]{0:T(128)} %get-tuple-element.385) | copy-start | bytes 100
  422.6 20.6 %copy-start.43 = (f32[8]{0:T(128)S(1)}, f32[8]{0:T(128)}, u32[]{:S(2)}) copy-start(f32[8]{0:T(128)} %get-tuple-element.386) | copy-start | bytes 100
  422.6 20.6 %copy-start.44 = (f32[8]{0:T(128)S(1)}, f32[8]{0:T(128)}, u32[]{:S(2)}) copy-start(f32[8]{0:T(128)} %get-tuple-element.387) | copy-start | bytes 100
  422.6 20.6 %copy-start.45 = (f32[8]{0:T(128)S(1)}, f32[8]{0:T(128)}, u32[]{:S(2)}) copy-start(f32[8]{0:T(128)} %get-tuple-element.388) | copy-start | bytes 100
  422.6 20.6 %copy-start.46 = (f32[8]{0:T(128)S(1)}, f32[8]{0:T(128)}, u32[]{:S(2)}) copy-start(f32[8]{0:T(128)} %get-tuple-element.389) | copy-start | bytes 100
  (33 other events, 347.2 us)
Sparse Core Ops, SparseCore 0:
  10.7 92.1 all-gather.11
  314.0 38.9 all-gather.15
  421.6 38.8 all-gather.13
where the time goes:
time: 528 us; the launch traced here: 523 us
  local copies, waits for them, and re-layouts  168 us (32%)
  blocking collectives  119 us (23%)
  waiting for transfers between devices  91.3 us (17%)
  matrix products  74.5 us (14%)
  other arithmetic  41 us (8%)
  between operations  15.4 us (3%)
  starting transfers between devices  11.2 us (2%)
    all_gather x1, waiting for transfers between devices, turned_gather(): out = lax.all_gather(both, axis, axis=0, tiled=True)  83.6 us
    all_gather x8, blocking collectives, carried_in(): lax.all_gather(part.astype(kind), axis)  79.8 us
    dynamic_update_slice x12, local copies, waits for them, and re-layouts, direction(): end_state, local = lax.scan(block_ssd, start_state, shaped)  76.7 us
    all_to_all x1, blocking collectives, sent_and_summed(): lax.all_to_all(parts, axis, split_axis=0, concat_axis=0, tiled=True)  36.8 us
    dynamic_slice x12, local copies, waits for them, and re-layouts, direction(): end_state, local = lax.scan(block_ssd, start_state, shaped)  22.4 us
    dot_general x5, matrix products, shards(): jnp.dot(normed, matrix, preferred_element_type=jnp.float32)  20.3 us
    another operation x20, local copies, waits for them, and re-layouts  18.8 us
    dot_general x12, matrix products, block_ssd(): jnp.einsum('lsh,shp->lhp', intersection * weight, xdt, precision=HIGH)  12.7 us
  transfers between devices with their start and end apart: 7, of which 2 were waited for; matrix products, arithmetic and copies ran while one was open for 49% of the time, Pallas kernels for 0%

commit v1 on v0

--- a/solution.py
+++ b/solution.py
@@ -20,7 +20,9 @@
     turned = [jnp.moveaxis(a, dim, 0) for a, dim in zip(arrays, dims)]
     widths = [t[0].size for t in turned]
     both = jnp.concatenate([t.reshape(-1, w) for t, w in zip(turned, widths)], axis=1)
-    out = lax.all_gather(both, axis, axis=0, tiled=True)
+    out = jnp.concatenate(
+        lax.all_to_all(jnp.stack([both] * lax.axis_size(axis)), axis, 0, 0), axis=0
+    )
     parts = jnp.split(out, [sum(widths[:k]) for k in range(1, len(widths))], axis=1)
     return tuple(
         (

time: 528 us -> 745 us (1.41)
  waiting for transfers between devices: 91.3 us -> 284 us
  starting transfers between devices: 11.2 us -> 23.6 us
    all_to_all x0 -> x1, waiting for transfers between devices: none -> 284 us  [turned_gather(): lax.all_to_all(jnp.stack([both] * lax.axis_size(axis)), axis, 0, 0)]
    all_gather x1 -> x0, waiting for transfers between devices: 83.6 us -> none  [turned_gather(): out = lax.all_gather(both, axis, axis=0, tiled=True)]
    all_to_all x0 -> x1, starting transfers between devices: none -> 12.4 us  [turned_gather(): lax.all_to_all(jnp.stack([both] * lax.axis_size(axis)), axis, 0, 0)]
    all_gather x2, waiting for transfers between devices: 7.54 us -> 0.01 us  [carried_in(): lax.all_gather(part.astype(kind), axis)]
    another operation x20 -> x21, local copies, waits for them, and re-layouts: 18.8 us -> 22.9 us
  transfers between devices with their start and end apart: 7 -> 7, of which waited for: 2 -> 1; matrix products, arithmetic and copies ran while one was open for 49% -> 33% of each run, Pallas kernels for 0% -> 0%
where the time goes in v1:
time: 745 us; the launch traced here: 738 us
  waiting for transfers between devices  284 us (38%)
  local copies, waits for them, and re-layouts  175 us (23%)
  blocking collectives  119 us (16%)
  matrix products  80.1 us (11%)
  other arithmetic  37.2 us (5%)
  starting transfers between devices  23.6 us (3%)
  between operations  15.8 us (2%)
    all_to_all x1, waiting for transfers between devices, turned_gather(): lax.all_to_all(jnp.stack([both] * lax.axis_size(axis)), axis, 0, 0)  284 us
    all_gather x8, blocking collectives, carried_in(): lax.all_gather(part.astype(kind), axis)  78.3 us
    dynamic_update_slice x12, local copies, waits for them, and re-layouts, direction(): end_state, local = lax.scan(block_ssd, start_state, shaped)  76.8 us
    all_to_all x1, blocking collectives, sent_and_summed(): lax.all_to_all(parts, axis, split_axis=0, concat_axis=0, tiled=True)  38.5 us
    dynamic_slice x12, local copies, waits for them, and re-layouts, direction(): end_state, local = lax.scan(block_ssd, start_state, shaped)  22.6 us
    dot_general x5, matrix products, shards(): jnp.dot(normed, matrix, preferred_element_type=jnp.float32)  19.4 us
    another operation x20, local copies, waits for them, and re-layouts  17.3 us
  transfers between devices with their start and end apart: 7, of which 1 were waited for; matrix products, arithmetic and copies ran while one was open for 33% of the time, Pallas kernels for 0%

profile of v1, /device:TPU:8, one launch (start us, length us, event | category | flops | bytes accessed | tf_op | source)
XLA Modules:
  0.0 738.3 jit_solution(17940003640860717334)
XLA Ops:
  9.7 5.6 stack.2
  15.4 12.4 %all-to-all-start = ((bf16[64,32,3088]{2,1,0:T(8,128)(2,1)}), bf16[64,32,3088]{2,1,0:T(8,128)(2,1)}, u32[]{:S(2)}, u32[]{:S(2)}) async-start(bf16[64,32,3088]{2,1,0:T(8,128)(2,1)} %stack.2), calls=%async_computation | async-start | bytes 26214400 | tf_op jit(solution)/shard_map/all_to_all | solution.py:24
  32.9 283.9 %all-to-all-done = bf16[64,32,3088]{2,1,0:T(8,128)(2,1)} async-done(((bf16[64,32,3088]{2,1,0:T(8,128)(2,1)}), bf16[64,32,3088]{2,1,0:T(8,128)(2,1)}, u32[]{:S(2)}, u32[]{:S(2)}) %all-to-all-start) | async-done | bytes 12648480 | tf_op jit(solution)/shard_map/all_to_all | solution.py:24
  316.7 5.6 fusion.101
  342.6 7.0 all-gather.4
  350.8 9.3 %all-gather.6 = bf16[4,1,8]{2,1,0:T(2,128)(2,1)S(1)} all-gather(bf16[1,1,8]{2,1,0:T(2,128)(2,1)S(1)} %get-tuple-element.405), channel_id=1, replica_groups=mesh['sp_0'=8,'sp_1'=4,'sp_2'=2,'tp'=4] {'sp_1'}, dimensions={0}, use_global_device_ids=true | all-gather | bytes 80 | tf_op jit(solution)/shard_map/all_gather | solution.py:47
  361.3 16.3 %all-gather.7 = bf16[8,1,8]{2,1,0:T(2,128)(2,1)S(1)} all-gather(bf16[1,1,8]{2,1,0:T(2,128)(2,1)S(1)} %get-tuple-element.396), channel_id=1, replica_groups=mesh['sp_0'=8,'sp_1'=4,'sp_2'=2,'tp'=4] {'sp_0'}, dimensions={0}, use_global_device_ids=true | all-gather | bytes 144 | tf_op jit(solution)/shard_map/all_gather | solution.py:47
  382.3 13.7 %all-gather.5 = bf16[8,1,8]{2,1,0:T(2,128)(2,1)S(1)} all-gather(bf16[1,1,8]{2,1,0:T(2,128)(2,1)S(1)} %get-tuple-element.391), channel_id=1, replica_groups=mesh['sp_0'=8,'sp_1'=4,'sp_2'=2,'tp'=4] {'sp_0'}, dimensions={0}, use_global_device_ids=true | all-gather | bytes 144 | tf_op jit(solution)/shard_map/all_gather | solution.py:47
  430.4 74.5 %while.42 = (s32[]{:T(128)}, f32[8,64,128]{2,1,0:T(8,128)S(1)}, f32[6,128,8,64]{1,0,3,2:T(8,128)S(1)}, f32[6,128,8]{2,1,0:T(8,128)}, f32[6,128,8,64]{1,0,3,2:T(8...) while((s32[]{:T(128)}, f32[8,64,128]{2,1,0:T(8,128)S(1)}, ...), condition=%wide.region_9.10_spmd.clone, body=%wide.region_7.9_spmd.clone.sunk | while | flops 156188672 | bytes 3768644 | solution.py:232
  449.7 5.1 dynamic_update_slice.32
  462.1 5.1 dynamic_update_slice.32
  474.5 5.1 dynamic_update_slice.32
  507.6 14.4 %all_gather.64 = bf16[4,8,64,128]{3,2,1,0:T(8,128)(2,1)S(1)} all-gather(bf16[1,8,64,128]{3,2,1,0:T(8,128)(2,1)S(1)} %fusion.172), channel_id=1, replica_groups=mesh['sp_0'=8,'sp_1'=4,'sp_2'=2,'tp'=4] {'sp_1'}, dimensions={0}, use_global_device_ids=true | all-gather | bytes 655360 | tf_op jit(solution)/shard_map/all_gather | solution.py:47
  529.0 80.3 %while.41 = (s32[]{:T(128)}, f32[8,64,128]{2,1,0:T(8,128)S(1)}, f32[6,128,8,64]{1,0,3,2:T(8,128)}, f32[6,128,8]{2,1,0:T(8,128)}, f32[6,128,8,64]{1,0,3,2:T(8,128...) while((s32[]{:T(128)}, f32[8,64,128]{2,1,0:T(8,128)S(1)}, ...), condition=%wide.region_3.4_spmd.clone, body=%wide.region_1.3_spmd.clone.sunk | while | flops 156188672 | bytes 3768644 | solution.py:232
  534.3 7.7 %dynamic_update_slice.31 = f32[6,128,8,64]{1,0,3,2:T(8,128)} dynamic-update-slice(f32[6,128,8,64]{1,0,3,2:T(8,128)} %get-tuple-element.665, f32[1,128,8,64]{1,0,3,2:T(1,128)S(1)} %bitcast.675, s32[]{:T(128)} %get-tuple-element.663, s32[]{:T(128)} %constant.172.clone.1..sunk.1, s32[]{:T(128)} %constant.172.clone.1..sunk.1, s32[]{:T(128)} %constant.172.clone.1..sunk.1) | dynamic-update-slice | bytes 524292 | tf_op jit(solution)/shard_map/while/body/jit(dynamic_update_index_in_dim)/dynamic_update_slice | solution.py:232
  547.7 7.7 %dynamic_update_slice.31 = f32[6,128,8,64]{1,0,3,2:T(8,128)} dynamic-update-slice(f32[6,128,8,64]{1,0,3,2:T(8,128)} %get-tuple-element.665, f32[1,128,8,64]{1,0,3,2:T(1,128)S(1)} %bitcast.675, s32[]{:T(128)} %get-tuple-element.663, s32[]{:T(128)} %constant.172.clone.1..sunk.1, s32[]{:T(128)} %constant.172.clone.1..sunk.1, s32[]{:T(128)} %constant.172.clone.1..sunk.1) | dynamic-update-slice | bytes 524292 | tf_op jit(solution)/shard_map/while/body/jit(dynamic_update_index_in_dim)/dynamic_update_slice | solution.py:232
  561.1 7.7 %dynamic_update_slice.31 = f32[6,128,8,64]{1,0,3,2:T(8,128)} dynamic-update-slice(f32[6,128,8,64]{1,0,3,2:T(8,128)} %get-tuple-element.665, f32[1,128,8,64]{1,0,3,2:T(1,128)S(1)} %bitcast.675, s32[]{:T(128)} %get-tuple-element.663, s32[]{:T(128)} %constant.172.clone.1..sunk.1, s32[]{:T(128)} %constant.172.clone.1..sunk.1, s32[]{:T(128)} %constant.172.clone.1..sunk.1) | dynamic-update-slice | bytes 524292 | tf_op jit(solution)/shard_map/while/body/jit(dynamic_update_index_in_dim)/dynamic_update_slice | solution.py:232
  574.5 7.7 %dynamic_update_slice.31 = f32[6,128,8,64]{1,0,3,2:T(8,128)} dynamic-update-slice(f32[6,128,8,64]{1,0,3,2:T(8,128)} %get-tuple-element.665, f32[1,128,8,64]{1,0,3,2:T(1,128)S(1)} %bitcast.675, s32[]{:T(128)} %get-tuple-element.663, s32[]{:T(128)} %constant.172.clone.1..sunk.1, s32[]{:T(128)} %constant.172.clone.1..sunk.1, s32[]{:T(128)} %constant.172.clone.1..sunk.1) | dynamic-update-slice | bytes 524292 | tf_op jit(solution)/shard_map/while/body/jit(dynamic_update_index_in_dim)/dynamic_update_slice | solution.py:232
  587.9 7.7 %dynamic_update_slice.31 = f32[6,128,8,64]{1,0,3,2:T(8,128)} dynamic-update-slice(f32[6,128,8,64]{1,0,3,2:T(8,128)} %get-tuple-element.665, f32[1,128,8,64]{1,0,3,2:T(1,128)S(1)} %bitcast.675, s32[]{:T(128)} %get-tuple-element.663, s32[]{:T(128)} %constant.172.clone.1..sunk.1, s32[]{:T(128)} %constant.172.clone.1..sunk.1, s32[]{:T(128)} %constant.172.clone.1..sunk.1) | dynamic-update-slice | bytes 524292 | tf_op jit(solution)/shard_map/while/body/jit(dynamic_update_index_in_dim)/dynamic_update_slice | solution.py:232
  601.3 7.7 %dynamic_update_slice.31 = f32[6,128,8,64]{1,0,3,2:T(8,128)} dynamic-update-slice(f32[6,128,8,64]{1,0,3,2:T(8,128)} %get-tuple-element.665, f32[1,128,8,64]{1,0,3,2:T(1,128)S(1)} %bitcast.675, s32[]{:T(128)} %get-tuple-element.663, s32[]{:T(128)} %constant.172.clone.1..sunk.1, s32[]{:T(128)} %constant.172.clone.1..sunk.1, s32[]{:T(128)} %constant.172.clone.1..sunk.1) | dynamic-update-slice | bytes 524292 | tf_op jit(solution)/shard_map/while/body/jit(dynamic_update_index_in_dim)/dynamic_update_slice | solution.py:232
  611.5 13.6 %all_gather.57 = bf16[4,8,64,128]{3,2,1,0:T(8,128)(2,1)S(1)} all-gather(bf16[1,8,64,128]{3,2,1,0:T(8,128)(2,1)S(1)} %fusion.168), channel_id=1, replica_groups=mesh['sp_0'=8,'sp_1'=4,'sp_2'=2,'tp'=4] {'sp_1'}, dimensions={0}, use_global_device_ids=true | all-gather | bytes 655360 | tf_op jit(solution)/shard_map/all_gather | solution.py:47
  631.5 31.5 %while.40 = (s32[]{:T(128)}, bf16[3,256,512]{2,1,0:T(8,128)(2,1)S(1)}, f32[3,256,8]{1,2,0:T(8,128)}, s32[3]{0:T(128)S(1)}, bf16[1024,256]{0,1:T(8,128)(2,1)S(1)}...) while((s32[]{:T(128)}, ...), condition=%wide.region_17.18_spmd, body=%wide.region_14.17_spmd.sunk | while | flops 280901888 | bytes 32392092 | solution.py:307
  682.5 8.7 %fusion.78 = bf16[768,2048]{1,0:T(8,128)(2,1)S(1)} fusion(bf16[2048,3088]{1,0:T(8,128)(2,1)} %bitcast.21, bf16[768,512]{0,1:T(8,128)(2,1)S(1)} %copy-done.12, bf16[768,512]{0,1:T(8,128)(2,1)S(1)} %multiply_convert_fusion.1), kind=kOutput, calls=%fused_computation.107 | convolution fusion | flops 3225944064 | bytes 8912896 | tf_op jit(solution)/shard_map/dot_general | solution.py:311
  691.4 38.5 %all_to_all.10 = bf16[4,768,512]{2,1,0:T(8,128)(2,1)S(1)} all-to-all(bf16[4,768,512]{2,1,0:T(8,128)(2,1)S(1)} %bitcast.678), channel_id=1, replica_groups=mesh['sp_0'=8,'sp_1'=4,'sp_2'=2,'tp'=4] {'tp'}, dimensions={0} | all-to-all | bytes 6291456 | tf_op jit(solution)/shard_map/all_to_all | solution.py:87
  (481 shorter events, 228.9 us)
Async XLA Ops:
  15.4 301.3 %all-to-all-start = ((bf16[64,32,3088]{2,1,0:T(8,128)(2,1)}), bf16[64,32,3088]{2,1,0:T(8,128)(2,1)}, u32[]{:S(2)}, u32[]{:S(2)}) async-start(bf16[64,32,3088]{2,1,0:T(8,128)(2,1)} %stack.2), calls=%async_computation | async-start | bytes 26214400 | tf_op jit(solution)/shard_map/all_to_all | solution.py:24
  27.8 636.4 %all-gather.13.cloned.1.call-start = ((), (), s32[]{:S(2)}) async-start(), calls=%async_computation.3 | async-start | bytes 1179648 | tf_op jit(solution)/shard_map/all_gather | solution.py:47
  32.4 303.2 %copy-start.21 = (f32[768]{0:T(1024)}, f32[768]{0:T(1024)S(1)}, u32[]{:S(2)}) copy-start(f32[768]{0:T(1024)S(1)} %add_rsqrt_fusion.1) | copy-start | bytes 9220
  330.1 80.3 %collective-permute-start = (bf16[2,768]{1,0:T(2,128)(2,1)S(1)}, bf16[2,768]{1,0:T(2,128)(2,1)S(1)}, u32[]{:S(2)}, u32[]{:S(2)}) collective-permute-start(bf16[2,768]{1,0:T(2,128)(2,1)S(1)} %get-tuple-element.353), channel_id=1, source_target_pairs={{0,4},{4,8},{8,12},{12,16},{16,20},{20,24},{24,28},{28,32},{32,36}... | collective-permute-start | bytes 9224 | tf_op jit(solution)/shard_map/ppermute | solution.py:70
  332.0 78.4 %collective-permute-start.1 = (bf16[2,768]{1,0:T(2,128)(2,1)S(1)}, bf16[2,768]{1,0:T(2,128)(2,1)S(1)}, u32[]{:S(2)}, u32[]{:S(2)}) collective-permute-start(bf16[2,768]{1,0:T(2,128)(2,1)S(1)} %get-tuple-element.354), channel_id=1, source_target_pairs={{4,0},{8,4},{12,8},{16,12},{20,16},{24,20},{28,24},{32,28},{36,32}... | collective-permute-start | bytes 9224 | tf_op jit(solution)/shard_map/ppermute | solution.py:72
  401.9 228.4 %collective-permute-start.2 = (bf16[128,256]{0,1:T(8,128)(2,1)}, bf16[128,256]{0,1:T(8,128)(2,1)}, u32[]{:S(2)}, u32[]{:S(2)}) collective-permute-start(bf16[128,256]{0,1:T(8,128)(2,1)} %get-tuple-element.359), channel_id=1, source_target_pairs={{0,4},{4,8},{8,12},{12,16},{16,20},{20,24},{24,28},{28,32},{32,36}... | collective-permute-start | bytes 196616 | tf_op jit(solution)/shard_map/ppermute | solution.py:70
  403.9 226.5 %collective-permute-start.3 = (bf16[128,256]{0,1:T(8,128)(2,1)}, bf16[128,256]{0,1:T(8,128)(2,1)}, u32[]{:S(2)}, u32[]{:S(2)}) collective-permute-start(bf16[128,256]{0,1:T(8,128)(2,1)} %get-tuple-element.360), channel_id=1, source_target_pairs={{4,0},{8,4},{12,8},{16,12},{20,16},{24,20},{28,24},{32,28},{36,32}... | collective-permute-start | bytes 196616 | tf_op jit(solution)/shard_map/ppermute | solution.py:72
  524.4 149.5 %all-gather.11.cloned.1.call-start = ((), (), s32[]{:S(2)}) async-start(), calls=%async_computation.2 | async-start | bytes 1179648 | tf_op jit(solution)/shard_map/all_gather | solution.py:47
  529.0 82.4 %copy-start.23 = (f32[8]{0:T(128)S(1)}, f32[8]{0:T(128)}, u32[]{:S(2)}) copy-start(f32[8]{0:T(128)} %get-tuple-element.401) | copy-start | bytes 100
  529.0 82.4 %copy-start.24 = (f32[8]{0:T(128)S(1)}, f32[8]{0:T(128)}, u32[]{:S(2)}) copy-start(f32[8]{0:T(128)} %get-tuple-element.403) | copy-start | bytes 100
  529.0 96.2 %copy-start.25 = (f32[8]{0:T(128)S(1)}, f32[8]{0:T(128)}, u32[]{:S(2)}) copy-start(f32[8]{0:T(128)} %get-tuple-element.392) | copy-start | bytes 100
  529.0 96.2 %copy-start.29 = (f32[8]{0:T(128)S(1)}, f32[8]{0:T(128)}, u32[]{:S(2)}) copy-start(f32[8]{0:T(128)} %get-tuple-element.393) | copy-start | bytes 100
  529.0 96.2 %copy-start.30 = (f32[8]{0:T(128)S(1)}, f32[8]{0:T(128)}, u32[]{:S(2)}) copy-start(f32[8]{0:T(128)} %get-tuple-element.394) | copy-start | bytes 100
  529.0 96.1 %copy-start.31 = (f32[8]{0:T(128)S(1)}, f32[8]{0:T(128)}, u32[]{:S(2)}) copy-start(f32[8]{0:T(128)} %get-tuple-element.395) | copy-start | bytes 100
  631.3 32.9 %copy-start.10 = (bf16[16,64,128]{2,1,0:T(8,128)(2,1)S(1)}, bf16[16,64,128]{2,1,0:T(8,128)(2,1)}, u32[]{:S(2)}) copy-start(bf16[16,64,128]{2,1,0:T(8,128)(2,1)} %copy-done.9) | copy-start | bytes 786436
  631.3 32.9 %copy-start.14 = (bf16[6,128,1,128]{3,1,2,0:T(8,128)(2,1)S(1)}, bf16[6,128,1,128]{3,1,2,0:T(8,128)(2,1)}, u32[]{:S(2)}) copy-start(bf16[6,128,1,128]{3,1,2,0:T(8,128)(2,1)} %copy-done.13) | copy-start | bytes 589828
  631.4 32.9 %copy-start.17 = (f32[768,8]{0,1:T(8,128)S(1)}, f32[768,8]{0,1:T(8,128)}, u32[]{:S(2)}) copy-start(f32[768,8]{0,1:T(8,128)} %exponential_bitcast_fusion) | copy-start | bytes 73732
  631.4 32.9 %copy-start.26 = (f32[8]{0:T(128)S(1)}, f32[8]{0:T(128)}, u32[]{:S(2)}) copy-start(f32[8]{0:T(128)} %get-tuple-element.404) | copy-start | bytes 100
  631.4 32.9 %copy-start.27 = (f32[8]{0:T(128)S(1)}, f32[8]{0:T(128)}, u32[]{:S(2)}) copy-start(f32[8]{0:T(128)} %get-tuple-element.406) | copy-start | bytes 100
  631.4 32.9 %copy-start.28 = (f32[8]{0:T(128)S(1)}, f32[8]{0:T(128)}, u32[]{:S(2)}) copy-start(f32[8]{0:T(128)} %get-tuple-element.397) | copy-start | bytes 100
  631.4 32.9 %copy-start.32 = (f32[8]{0:T(128)S(1)}, f32[8]{0:T(128)}, u32[]{:S(2)}) copy-start(f32[8]{0:T(128)} %get-tuple-element.398) | copy-start | bytes 100
  631.4 32.9 %copy-start.33 = (f32[8]{0:T(128)S(1)}, f32[8]{0:T(128)}, u32[]{:S(2)}) copy-start(f32[8]{0:T(128)} %get-tuple-element.399) | copy-start | bytes 100
  631.4 32.9 %copy-start.34 = (f32[8]{0:T(128)S(1)}, f32[8]{0:T(128)}, u32[]{:S(2)}) copy-start(f32[8]{0:T(128)} %get-tuple-element.400) | copy-start | bytes 100
  631.4 32.9 %copy-start.47 = (f32[8]{0:T(128)S(1)}, f32[8]{0:T(128)}, u32[]{:S(2)}) copy-start(f32[8]{0:T(128)} %get-tuple-element.329) | copy-start | bytes 100
  (46 other events, 559.6 us)
Sparse Core Ops, SparseCore 0:
  524.5 39.0 all-gather.12
  630.4 39.2 all-gather.10
